TPU v7x, 32 devices: a whole 2x2x4 slice. The times are simulated.
32 devices in a mesh: gr: 2 (over y), sp: 4 (over z), tp: 4 (over x, core).
Axes of the slice: x: 2, y: 2, z: 4, core: 2. Of those that a mesh axis runs over, the one named last changes fastest.
Arguments:
- tokens: bfloat16 [4, 1024, 4096], P('gr', ('sp', 'tp')), parts along dimension 0, may hold values from -6 to 6
- norm_gain: bfloat16 [4096], replicated, may hold values from 0.099609375 to 1.8984375
- key_weight: bfloat16 [4096, 1024], P(None, 'tp'), may hold values from -0.09375 to 0.09375
- value_weight: bfloat16 [4096, 1024], P(None, 'tp'), may hold values from -0.09375 to 0.09375
- cum_gates: float32 [4, 1024, 16], P('gr', 'sp', 'tp'), parts along dimension 0, may hold values from -173 to 0, as said below
- new_query: bfloat16 [4, 1024], P('gr', 'tp'), parts along dimension 0, may hold values from -240 to 240
- new_key: bfloat16 [4, 1024], P('gr', 'tp'), parts along dimension 0, may hold values from -6 to 6
- new_value: bfloat16 [4, 1024], P('gr', 'tp'), parts along dimension 0, may hold values from -6 to 6
- new_gate: float32 [4, 16], P('gr', 'tp'), parts along dimension 0, may hold values from -5 to -1.5
Outputs:
- key_cache: bfloat16 [4, 1024, 1024], P('gr', 'sp', 'tp'), parts along dimension 0
- value_cache: bfloat16 [4, 1024, 1024], P('gr', 'sp', 'tp'), parts along dimension 0
- readout: bfloat16 [4, 1024], P('gr', 'tp'), parts along dimension 0
There are 2 independent parts, one for each index of `gr`. A program takes and returns all parts, laid end to end along the dimension named above; an argument that names none is the same for every part. Nothing has to cross between parts.
Inputs may be any that keep to these rules, and one draw needn't show every extreme that they name: `cum_gates`: along positions, for each prompt and head, the values never rise.
All inputs are finite; a program needn't handle non-finite values.
Results may differ from a plain program's by a relative error of at most 0.005.
The roundings to bfloat16 on the way count: a program that leaves them out, or rounds other values in their place, can miss the bound.
Values may be sent and summed in bfloat16 or wider, within the bound.
A program may use at most 64 MiB of HBM per device.

v0:
```python
import jax
import jax.numpy as jnp
from jax import lax
from jax.sharding import PartitionSpec as P

HD = 64


epsilon = 1e-06
masked_score = -1e30


def body(
    tokens, norm_gain, key_weight, value_weight, cum_gates, new_query, new_key, new_value, new_gate
):
    seq_count, own_len, model_width = tokens.shape
    as_float = tokens.astype(jnp.float32)
    normed = (
        as_float
        * lax.rsqrt(jnp.mean(as_float * as_float, axis=-1, keepdims=True) + epsilon)
        * norm_gain.astype(jnp.float32)
    ).astype(jnp.bfloat16)
    key_width = key_weight.shape[1]
    local_heads = key_width // HD
    both_weights = jnp.concatenate([key_weight, value_weight], axis=1)
    piece = lax.all_gather(normed, "tp", axis=1, tiled=True)
    piece_len = piece.shape[1]
    rows = piece.reshape(seq_count * piece_len, model_width)
    result = jnp.dot(rows, both_weights, preferred_element_type=jnp.float32).astype(jnp.bfloat16)
    projected = result.reshape(seq_count, piece_len, 2 * key_width)
    key_cache = projected[:, :, :key_width]
    value_cache = projected[:, :, key_width:]
    block_len = projected.shape[1]
    sp_count = lax.axis_size("sp")
    sp_index = lax.axis_index("sp")
    score_scale = HD ** (-0.5)
    queries = new_query.reshape(seq_count, local_heads, HD)
    fresh_key = new_key.reshape(seq_count, local_heads, HD).astype(jnp.float32)
    fresh_value = new_value.reshape(seq_count, local_heads, HD).astype(jnp.float32)
    fresh_score = jnp.sum(queries.astype(jnp.float32) * fresh_key, axis=-1) * score_scale
    key_heads = key_cache.reshape(seq_count, block_len, local_heads, HD)
    value_heads = value_cache.reshape(seq_count, block_len, local_heads, HD).astype(jnp.float32)
    scores = (
        jnp.einsum("shd,slhd->shl", queries, key_heads, preferred_element_type=jnp.float32)
        * score_scale
    )
    scores = scores - jnp.transpose(cum_gates, (0, 2, 1))
    last_block = sp_index == sp_count - 1
    fresh_term = jnp.where(
        last_block, fresh_score - (cum_gates[:, block_len - 1, :] + new_gate), masked_score
    )
    local_top = jnp.maximum(jnp.max(scores, axis=-1), fresh_term)
    maxima = lax.pmax(local_top, "sp")
    weights = jnp.exp(scores - maxima[:, :, None])
    fresh_weight = jnp.exp(fresh_term - maxima)
    totals = jnp.sum(weights, axis=-1) + fresh_weight
    weighted = jnp.einsum("shl,slhd->shd", weights, value_heads, precision=lax.Precision.HIGHEST)
    weighted = weighted + fresh_weight[:, :, None] * fresh_value
    totals, weighted = lax.psum((totals, weighted), "sp")
    readout = (weighted / totals[:, :, None]).reshape(seq_count, key_width).astype(jnp.bfloat16)
    return (key_cache, value_cache, readout)


def solution(mesh):
    in_specs = (
        P("gr", ("sp", "tp"), None),
        P(),
        P(None, "tp"),
        P(None, "tp"),
        P("gr", "sp", "tp"),
        P("gr", "tp"),
        P("gr", "tp"),
        P("gr", "tp"),
        P("gr", "tp"),
    )
    out_specs = (P("gr", "sp", "tp"), P("gr", "sp", "tp"), P("gr", "tp"))
    return jax.shard_map(body, mesh=mesh, in_specs=in_specs, out_specs=out_specs, check_vma=False)
```

profile of v0, /device:TPU:0, one launch (start us, length us, event | category | flops | bytes accessed | tf_op | source)
XLA Modules:
  0.0 83.7 jit_solution(6548077247722289311)
XLA Ops:
  7.2 0.0 all-gather.2.cloned.1.call-start
  7.2 0.7 convert_element_type.35
  7.9 0.0 copy-start.3
  7.9 0.0 copy-start.4
  7.9 0.0 copy-start.5
  7.9 0.0 copy-start.2
  7.9 0.0 copy-start.7
  7.9 1.7 %fusion.4 = f32[2,64]{1,0:T(2,128)S(1)} fusion(bf16[2,64,4096]{2,1,0:T(8,128)(2,1)} %param.9), kind=kLoop, calls=%fused_computation.6 | loop fusion | flops 1572736 | bytes 1049088 | tf_op jit(solution)/shard_map/reduce_sum | solution.py:20
  9.6 2.5 %fusion.6 = bf16[2,64,4096]{2,1,0:T(8,128)(2,1)} fusion(bf16[2,64,4096]{2,1,0:T(8,128)(2,1)} %param.9, f32[4096]{0:T(1024)S(1)} %convert_element_type.35, f32[2,64]{1,0:T(2,128)S(1)} %add_rsqrt_fusion), kind=kLoop, calls=%fused_computation.8 | loop fusion | flops 2097152 | bytes 2114048 | tf_op jit(solution)/shard_map/convert_element_type | solution.py:22
  12.2 0.0 all-gather.2.cloned.1.call-update
  12.2 0.0 copy-done.3
  12.2 0.1 reshape.53
  12.3 0.1 reshape.44
  12.4 0.0 copy-done.4
  12.4 0.1 reshape.46
  12.4 0.0 copy-done.5
  12.4 0.1 reshape.47
  12.5 0.0 copy-done.2
  12.5 0.2 slice_reduce_fusion
  12.7 0.1 multiply_reduce_fusion
  12.8 36.7 %all-gather.2.cloned.1.call-done = bf16[2,256,4096]{2,1,0:T(8,128)(2,1)} async-done(((bf16[2,64,4096]{2,1,0:T(8,128)(2,1)}), bf16[2,256,4096]{2,1,0:T(8,128)(2,1)}) %all-gather.2.cloned.1.call-update) | async-done | bytes 4194320 | tf_op jit(solution)/shard_map/all_gather | solution.py:26
  49.5 0.0 copy-done.7
  49.5 0.0 copy-start.6
  49.5 5.2 %fusion.7 = bf16[512,512]{1,0:T(8,128)(2,1)S(1)} fusion(bf16[512,4096]{1,0:T(8,128)(2,1)} %bitcast.34, bf16[4096,256]{1,0:T(8,128)(2,1)S(1)} %copy-done.7, bf16[4096,256]{1,0:T(8,128)(2,1)} %param.11), kind=kOutput, calls=%fused_computation.9 | convolution fusion | flops 2156134400 | bytes 8912896 | tf_op jit(solution)/shard_map/dot_general | solution.py:29
  54.8 0.0 copy-start
  54.8 0.0 copy-start.1
  54.8 0.1 copy.20
  55.0 0.1 fusion.19
  55.1 0.1 fusion.15
  55.2 0.0 copy-done.6
  55.2 11.7 %pmax.7 = f32[2,4]{1,0:T(2,128)S(1)} all-reduce(f32[2,4]{1,0:T(2,128)S(1)} %get-tuple-element.10), channel_id=1, replica_groups=mesh['gr'=2,'sp'=4,'tp'=4] {'sp'}, use_global_device_ids=true, to_apply=%region_3.4 | all-reduce | flops 8 | bytes 64 | tf_op jit(solution)/shard_map/pmax | solution.py:53
  66.9 0.2 fusion.12
  67.1 0.1 copy.21
  67.2 0.3 fusion.10
  67.5 0.1 multiply_add_fusion
  67.6 8.5 %all-reduce = (f32[2,4,64]{2,1,0:T(4,128)S(1)}, f32[2,4]{1,0:T(2,128)S(1)}) all-reduce(f32[2,4,64]{2,1,0:T(4,128)S(1)} %multiply_add_fusion, f32[2,4]{1,0:T(2,128)S(1)} %get-tuple-element.8), channel_id=1, replica_groups=mesh['gr'=2,'sp'=4,'tp'=4] {'sp'}, use_global_device_ids=true, to_apply=%region_4.5 | all-reduce | flops 520 | bytes 4160 | tf_op jit(solution)/shard_map/psum | solution.py:59
  76.1 0.1 divide_convert_fusion
  76.2 0.7 convert_element_type.44
  76.9 0.0 copy-done
  76.9 0.0 copy-done.1
  (4 shorter events, 0.1 us)
Async XLA Ops:
  7.2 42.3 %all-gather.2.cloned.1.call-start = ((), (), s32[]{:S(2)}) async-start(), calls=%async_computation | async-start | bytes 5242880 | tf_op jit(solution)/shard_map/all_gather | solution.py:26
  7.9 4.3 %copy-start.3 = (bf16[2,256]{1,0:T(2,128)(2,1)S(1)}, bf16[2,256]{1,0:T(2,128)(2,1)}, u32[]{:S(2)}) copy-start(bf16[2,256]{1,0:T(2,128)(2,1)} %param.14) | copy-start | bytes 3076
  7.9 4.4 %copy-start.4 = (bf16[2,256]{1,0:T(2,128)(2,1)S(1)}, bf16[2,256]{1,0:T(2,128)(2,1)}, u32[]{:S(2)}) copy-start(bf16[2,256]{1,0:T(2,128)(2,1)} %param.15) | copy-start | bytes 3076
  7.9 4.5 %copy-start.5 = (bf16[2,256]{1,0:T(2,128)(2,1)S(1)}, bf16[2,256]{1,0:T(2,128)(2,1)}, u32[]{:S(2)}) copy-start(bf16[2,256]{1,0:T(2,128)(2,1)} %param.16) | copy-start | bytes 3076
  7.9 4.6 %copy-start.2 = (f32[2,256,4]{1,2,0:T(4,128)S(1)}, f32[2,256,4]{1,2,0:T(4,128)}, u32[]{:S(2)}) copy-start(f32[2,256,4]{1,2,0:T(4,128)} %param.13) | copy-start | bytes 24580
  7.9 41.6 %copy-start.7 = (bf16[4096,256]{1,0:T(8,128)(2,1)S(1)}, bf16[4096,256]{1,0:T(8,128)(2,1)}, u32[]{:S(2)}) copy-start(bf16[4096,256]{1,0:T(8,128)(2,1)} %param.12) | copy-start | bytes 6291460
  49.5 5.7 %copy-start.6 = (f32[2,4]{1,0:T(2,128)S(1)}, f32[2,4]{1,0:T(2,128)}, u32[]{:S(2)}) copy-start(f32[2,4]{1,0:T(2,128)} %param.17) | copy-start | bytes 100
  54.8 22.1 %copy-start = (bf16[2,256,256]{2,1,0:T(8,128)(2,1)}, bf16[2,256,256]{2,1,0:T(8,128)(2,1)S(1)}, u32[]{:S(2)}) copy-start(bf16[2,256,256]{2,1,0:T(8,128)(2,1)S(1)} %get-tuple-element.12) | copy-start | bytes 786436
  54.8 22.0 %copy-start.1 = (bf16[2,256,256]{2,1,0:T(8,128)(2,1)}, bf16[2,256,256]{2,1,0:T(8,128)(2,1)S(1)}, u32[]{:S(2)}) copy-start(bf16[2,256,256]{2,1,0:T(8,128)(2,1)S(1)} %get-tuple-element.13) | copy-start | bytes 786436
Sparse Core Ops, SparseCore 0:
  12.3 37.1 all-gather.1
where the time goes:
time: 84 us; the launch traced here: 83.7 us
  waiting for transfers between devices  36.8 us (44%)
  blocking collectives  20.2 us (24%)
  between operations  14.1 us (17%)
  matrix products  5.69 us (7%)
  other arithmetic  5.42 us (6%)
  local copies, waits for them, and re-layouts  1.48 us (2%)
    all_gather x1, waiting for transfers between devices, body(): piece = lax.all_gather(normed, 'tp', axis=1, tiled=True)  36.7 us
    pmax x1, blocking collectives, body(): maxima = lax.pmax(local_top, 'sp')  11.7 us
    psum x1, blocking collectives, body(): totals, weighted = lax.psum((totals, weighted), 'sp')  8.5 us
    dot_general x1, matrix products, body(): jnp.dot(rows, both_weights, preferred_element_type=jnp.float32)  5.24 us
    convert_element_type x1, other arithmetic, body(): normed = (as_float * lax.rsqrt(jnp.mean(as_float * as_float, axis=-1, kee...  2.53 us
  transfers between devices with their start and end apart: 1, of which 1 were waited for; matrix products, arithmetic and copies ran while one was open for 1% of the time, Pallas kernels for 0%

commit v1 on v0

v1 whole, which is shorter than its diff:
```python
import functools

import jax
import jax.numpy as jnp
from jax import lax
from jax.experimental import pallas as pl
from jax.experimental.pallas import tpu as pltpu
from jax.sharding import PartitionSpec as P

HD = 64
CORES = 2

epsilon = 1e-06
masked_score = -1e30
MESH = pl.DeviceIdType.MESH


def kernel(
    dims,
    tok_hbm, gain_hbm, wk_hbm, wv_hbm, gates_hbm, q_hbm, nk_hbm, nv_hbm, ng_hbm,
    kc_hbm, vc_hbm, ro_ref,
    raw, nbuf, wbuf, kbuf, vbuf, gain_v, gates_v, q_v, nk_v, nv_v, ng_v, stats,
    loc_sem, w_sem, small_sem, out_sem,
    sx_sem, rx_sem, sp_sem, rp_sem, sr_sem, rr_sem, sz_sem, rz_sem,
):
    S, L, R, T, Z = dims
    X = T // CORES
    per = L // R
    NC = S * per
    C = kbuf.shape[2]
    H = C // HD
    BL = T * L
    tp = lax.axis_index("tp")
    z = lax.axis_index("sp")
    x, c = tp // CORES, tp % CORES
    partner = x * CORES + (CORES - 1 - c)

    def rows(j):
        return pl.ds(pl.multiple_of(j * R, R), R)

    for j in range(NC):
        pltpu.make_async_copy(tok_hbm.at[rows(j)], raw.at[tp, rows(j)], loc_sem.at[j]).start()
    w_copies = [
        pltpu.make_async_copy(wk_hbm, wbuf.at[:, pl.ds(0, C)], w_sem.at[0]),
        pltpu.make_async_copy(wv_hbm, wbuf.at[:, pl.ds(C, C)], w_sem.at[1]),
    ]
    small = [
        pltpu.make_async_copy(src, dst, small_sem.at[i])
        for i, (src, dst) in enumerate(
            [(gain_hbm, gain_v), (gates_hbm, gates_v), (q_hbm, q_v), (nk_hbm, nk_v), (nv_hbm, nv_v), (ng_hbm, ng_v)]
        )
    ]
    for copy in small + w_copies:
        copy.start()

    barrier = pltpu.get_barrier_semaphore()
    pl.semaphore_signal(barrier, inc=1, device_id={"tp": partner}, device_id_type=MESH)
    for d in range(1, X):
        pl.semaphore_signal(
            barrier, inc=1, device_id={"tp": ((x + d) % X) * CORES + c}, device_id_type=MESH
        )
    for d in range(1, Z):
        pl.semaphore_signal(barrier, inc=1, device_id={"sp": (z + d) % Z}, device_id_type=MESH)
    pl.semaphore_wait(barrier, 1 + (X - 1) + (Z - 1))

    def x_copy(d, j):
        return pltpu.make_async_remote_copy(
            raw.at[tp, rows(j)], raw.at[tp, rows(j)], sx_sem.at[d - 1, j], rx_sem.at[d - 1, j],
            device_id={"tp": ((x + d) % X) * CORES + c}, device_id_type=MESH,
        )

    def x_source(d, core):
        return ((x + X - d) % X) * CORES + core

    def relay_copy(d, j):
        t = x_source(d, c)
        return pltpu.make_async_remote_copy(
            raw.at[t, rows(j)], raw.at[t, rows(j)], sr_sem.at[d - 1, j], rr_sem.at[d - 1, j],
            device_id={"tp": partner}, device_id_type=MESH,
        )

    def arrival(t, j, sem):
        return pltpu.make_async_remote_copy(
            raw.at[t, rows(j)], raw.at[t, rows(j)], sem, sem,
            device_id={"tp": partner}, device_id_type=MESH,
        )

    for j in range(NC):
        pltpu.make_async_copy(tok_hbm.at[rows(j)], raw.at[tp, rows(j)], loc_sem.at[j]).wait()
        for d in range(1, X):
            x_copy(d, j).start()
    own_to_partner = pltpu.make_async_remote_copy(
        raw.at[tp], raw.at[tp], sp_sem, rp_sem, device_id={"tp": partner}, device_id_type=MESH
    )
    own_to_partner.start()

    for copy in small:
        copy.wait()
    gain = gain_v[...].astype(jnp.float32)

    def norm_into(t, j, at):
        v = raw[t, rows(j), :].astype(jnp.float32)
        r = lax.rsqrt(jnp.mean(v * v, axis=-1, keepdims=True) + epsilon)
        nbuf[pl.ds(pl.multiple_of(at, R), R), :] = (v * r * gain).astype(jnp.bfloat16)

    def project(count):
        return jnp.dot(
            nbuf[pl.ds(0, count), :], wbuf[...], preferred_element_type=jnp.float32
        ).astype(jnp.bfloat16)

    def keep(y, t, s, row, count):
        at = pl.ds(pl.multiple_of(t * L + row, R), count)
        kbuf[s, at, :] = y[:, :C]
        vbuf[s, at, :] = y[:, C:]

    def whole_source(t):
        def one(j, carry):
            norm_into(t, j, j * R)
            return carry

        lax.fori_loop(0, NC, one, 0)
        y = project(S * L)
        for s in range(S):
            keep(y[s * L : (s + 1) * L], t, s, 0, L)

    def near(i, carry):
        @pl.when(i == 1)
        def _():
            pltpu.make_async_remote_copy(
                raw.at[partner], raw.at[partner], sp_sem, rp_sem, device_id={"tp": partner}, device_id_type=MESH
            ).wait_recv()

        whole_source(x * CORES + (c + i) % CORES)
        return carry

    for copy in w_copies:
        copy.wait()
    lax.fori_loop(0, CORES, near, 0)

    def far(j, carry):
        for d in range(1, X):
            arrival(x_source(d, c), j, rx_sem.at[d - 1, j]).wait_recv()
            relay_copy(d, j).start()
        for d in range(1, X):
            norm_into(x_source(d, c), j, (d - 1) * R)
        for d in range(1, X):
            arrival(x_source(d, CORES - 1 - c), j, rr_sem.at[d - 1, j]).wait_recv()
            norm_into(x_source(d, CORES - 1 - c), j, (X - 1 + d - 1) * R)
        y = project(2 * (X - 1) * R)
        s, row = j // per, (j % per) * R
        for d in range(1, X):
            a, b = (d - 1) * R, (X - 1 + d - 1) * R
            keep(y[a : a + R], x_source(d, c), s, row, R)
            keep(y[b : b + R], x_source(d, CORES - 1 - c), s, row, R)
        return carry

    if X > 1:
        lax.fori_loop(0, NC, far, 0)

    outs = [
        pltpu.make_async_copy(kbuf, kc_hbm, out_sem.at[0]),
        pltpu.make_async_copy(vbuf, vc_hbm, out_sem.at[1]),
    ]
    for copy in outs:
        copy.start()

    scale = HD ** (-0.5)
    head_of_lane = lax.broadcasted_iota(jnp.int32, (H, C), 1) // HD
    own_head = head_of_lane == lax.broadcasted_iota(jnp.int32, (H, C), 0)
    eye = lax.broadcasted_iota(jnp.int32, (H, H), 0) == lax.broadcasted_iota(jnp.int32, (H, H), 1)
    last_block = z == Z - 1

    def as_row(column):
        return jnp.sum(jnp.where(own_head, column, 0.0), axis=0, keepdims=True)

    for s in range(S):
        qd = jnp.where(own_head, q_v[s : s + 1, :].astype(jnp.float32), 0.0)
        fresh = jnp.sum(qd * nk_v[s : s + 1, :].astype(jnp.float32), axis=1, keepdims=True) * scale
        gates = gates_v[s]
        own_gate = jnp.sum(jnp.where(eye, ng_v[s : s + 1, :], 0.0), axis=1, keepdims=True)
        fresh = jnp.where(last_block, fresh - (gates[:, BL - 1 : BL] + own_gate), masked_score)
        scores = lax.dot_general(
            qd.astype(jnp.bfloat16), kbuf[s], (((1,), (1,)), ((), ())), preferred_element_type=jnp.float32
        )
        scores = scores * scale - gates
        top = jnp.maximum(jnp.max(scores, axis=1, keepdims=True), fresh)
        weights = jnp.exp(scores - top)
        fresh_weight = jnp.exp(fresh - top)
        total = jnp.sum(weights, axis=1, keepdims=True) + fresh_weight
        high = weights.astype(jnp.bfloat16)
        low = (weights - high.astype(jnp.float32)).astype(jnp.bfloat16)
        values = vbuf[s]
        weighted = jnp.dot(high, values, preferred_element_type=jnp.float32)
        weighted = weighted + jnp.dot(low, values, preferred_element_type=jnp.float32)
        weighted = weighted + fresh_weight * nv_v[s : s + 1, :].astype(jnp.float32)
        stats[z, 0, s : s + 1, :] = as_row(top)
        stats[z, 1, s : s + 1, :] = as_row(total)
        stats[z, 2, s : s + 1, :] = as_row(weighted)

    def z_copy(d):
        return pltpu.make_async_remote_copy(
            stats.at[z], stats.at[z], sz_sem.at[d - 1], rz_sem.at[d - 1],
            device_id={"sp": (z + d) % Z}, device_id_type=MESH,
        )

    for d in range(1, Z):
        z_copy(d).start()
    for d in range(1, X):
        for j in range(NC):
            x_copy(d, j).wait_send()
            relay_copy(d, j).wait_send()
    own_to_partner.wait_send()
    for d in range(1, Z):
        source = (z + Z - d) % Z
        pltpu.make_async_remote_copy(
            stats.at[source], stats.at[source], sz_sem.at[d - 1], rz_sem.at[d - 1],
            device_id={"sp": source}, device_id_type=MESH,
        ).wait_recv()
    everything = stats[...]
    tops, totals, sums = everything[:, 0], everything[:, 1], everything[:, 2]
    factor = jnp.exp(tops - jnp.max(tops, axis=0, keepdims=True))
    ro_ref[...] = (jnp.sum(sums * factor, axis=0) / jnp.sum(totals * factor, axis=0)).astype(ro_ref.dtype)
    for d in range(1, Z):
        z_copy(d).wait_send()
    for copy in outs:
        copy.wait()


def body(
    tokens, norm_gain, key_weight, value_weight, cum_gates, new_query, new_key, new_value, new_gate
):
    S, L, D = tokens.shape
    C = key_weight.shape[1]
    H = C // HD
    T = lax.axis_size("tp")
    Z = lax.axis_size("sp")
    X = T // CORES
    BL = T * L
    R = 16 if L % 16 == 0 else L
    NC = S * (L // R)
    bf, f32 = jnp.bfloat16, jnp.float32
    hbm = pl.BlockSpec(memory_space=pltpu.HBM)
    dma = pltpu.SemaphoreType.DMA
    far = max(X - 1, 1)
    return pl.pallas_call(
        functools.partial(kernel, (S, L, R, T, Z)),
        out_shape=(
            jax.ShapeDtypeStruct((S, BL, C), bf),
            jax.ShapeDtypeStruct((S, BL, C), bf),
            jax.ShapeDtypeStruct((S, C), bf),
        ),
        in_specs=[hbm] * 9,
        out_specs=(hbm, hbm, pl.BlockSpec(memory_space=pltpu.VMEM)),
        scratch_shapes=[
            pltpu.VMEM((T, S * L, D), bf),
            pltpu.VMEM((max(S * L, 2 * far * R), D), bf),
            pltpu.VMEM((D, 2 * C), bf),
            pltpu.VMEM((S, BL, C), bf),
            pltpu.VMEM((S, BL, C), bf),
            pltpu.VMEM((1, D), bf),
            pltpu.VMEM((S, H, BL), f32),
            pltpu.VMEM((S, C), bf),
            pltpu.VMEM((S, C), bf),
            pltpu.VMEM((S, C), bf),
            pltpu.VMEM((S, H), f32),
            pltpu.VMEM((Z, 3, S, C), f32),
            dma((NC,)), dma((2,)), dma((6,)), dma((2,)),
            dma((far, NC)), dma((far, NC)), dma, dma,
            dma((far, NC)), dma((far, NC)), dma((max(Z - 1, 1),)), dma((max(Z - 1, 1),)),
        ],
        compiler_params=pltpu.CompilerParams(
            collective_id=0, has_side_effects=True, vmem_limit_bytes=56 * 1024 * 1024
        ),
    )(
        tokens.reshape(S * L, D),
        norm_gain.reshape(1, D),
        key_weight,
        value_weight,
        jnp.transpose(cum_gates, (0, 2, 1)),
        new_query,
        new_key,
        new_value,
        new_gate,
    )


def solution(mesh):
    in_specs = (
        P("gr", ("sp", "tp"), None),
        P(),
        P(None, "tp"),
        P(None, "tp"),
        P("gr", "sp", "tp"),
        P("gr", "tp"),
        P("gr", "tp"),
        P("gr", "tp"),
        P("gr", "tp"),
    )
    out_specs = (P("gr", "sp", "tp"), P("gr", "sp", "tp"), P("gr", "tp"))
    return jax.shard_map(body, mesh=mesh, in_specs=in_specs, out_specs=out_specs, check_vma=False)
```

time: 84 us -> 42.7 us (0.51)
  waiting for transfers between devices: 36.8 us -> 0 us
  Pallas kernels: 0 us -> 36 us
  blocking collectives: 20.2 us -> 0 us
  between operations: 14.1 us -> 0.64 us
  matrix products: 5.69 us -> 0 us
  other arithmetic: 5.42 us -> 0 us
  local copies, waits for them, and re-layouts: 1.48 us -> 5.85 us
    all_gather x1 -> x0, waiting for transfers between devices: 36.7 us -> none  [body(): piece = lax.all_gather(normed, 'tp', axis=1, tiled=True)]
    pallas_call x0 -> x1, Pallas kernels: none -> 36 us  [body(): pl.pallas_call(functools.partial(kernel, (S, L, R, T, Z)), out_shape=(jax...]
    pmax x1 -> x0, blocking collectives: 11.7 us -> none  [body(): maxima = lax.pmax(local_top, 'sp')]
    psum x1 -> x0, blocking collectives: 8.5 us -> none  [body(): totals, weighted = lax.psum((totals, weighted), 'sp')]
    dot_general x3 -> x0, matrix products: 5.69 us -> none  [the longest x1 5.24 us: body(): jnp.dot(rows, both_weights, preferred_element_type=jnp.float32)]
    unnamed x18 -> x3, local copies, waits for them, and re-layouts: 0.3 us -> 4.54 us
    convert_element_type x3 -> x0, other arithmetic: 3.31 us -> none  [the longest x1 2.53 us: body(): normed = (as_float * lax.rsqrt(jnp.mean(as_float * as_float, axis=-1, kee...]
    reduce_sum x3 -> x0, other arithmetic: 1.92 us -> none  [the longest x1 1.67 us: body(): jnp.mean(as_float * as_float, axis=-1, keepdims=True) + epsilon]
  transfers between devices with their start and end apart: 1 -> 0, of which waited for: 1 -> 0; matrix products, arithmetic and copies ran while one was open for 1% -> 0% of each run, Pallas kernels for 0% -> 0%
where the time goes in v1:
time: 42.7 us; the launch traced here: 42.5 us
  Pallas kernels  36 us (84%)
  local copies, waits for them, and re-layouts  5.85 us (14%)
  between operations  0.64 us (1%)
    pallas_call x1, Pallas kernels, body(): pl.pallas_call(functools.partial(kernel, (S, L, R, T, Z)), out_shape=(jax...  36 us
    unnamed x3, local copies, waits for them, and re-layouts  4.54 us
    reshape x1, local copies, waits for them, and re-layouts, body(): norm_gain.reshape(1, D)  1.31 us

profile of v1, /device:TPU:0, one launch (start us, length us, event | category | flops | bytes accessed | tf_op | source)
XLA Modules:
  0.0 42.5 jit_solution(6824709863450127136)
XLA Ops:
  0.6 1.3 %reshape.13.gain_hbm = bf16[1,4096]{1,0:T(2,128)(2,1)} reshape(bf16[4096]{0:T(1024)(128)(2,1)} %param.10) | data formatting | bytes 16384 | tf_op jit(solution)/shard_map/reshape | solution.py:276
  1.9 36.0 %shard_map.112 = (bf16[2,256,256]{2,1,0:T(8,128)(2,1)}, bf16[2,256,256]{2,1,0:T(8,128)(2,1)}, bf16[2,256]{1,0:T(2,128)(2,1)}) custom-call(bf16[128,4096]{1,0:T(8,128)(2,1)} %bitcast.2, bf16[1,4096]{1,0:T(2,128)(2,1)} %reshape.13.gain_hbm, bf16[4096,256]{1,0:T(8,128)(2,1)} %wk_hbm.1, bf16[4096,256]{1,0:T(8,128)(2,1)} %wv_hbm.1, f32[2,4,256]{2,1,0:T(4,128)} %bitcast.3, ...), custom_call_target="tpu_custom_call" | custom-call | tf_op jit(solution)/shard_map/pallas_call | solution.py:245
  37.9 1.7 %copy.15 = bf16[2,256,256]{2,1,0:T(8,128)(2,1)} copy(bf16[2,256,256]{2,1,0:T(8,128)(2,1)} %get-tuple-element.6) | data formatting | bytes 524288
  39.6 1.7 %copy.16 = bf16[2,256,256]{2,1,0:T(8,128)(2,1)} copy(bf16[2,256,256]{2,1,0:T(8,128)(2,1)} %get-tuple-element.7) | data formatting | bytes 524288
  41.3 1.2 %copy.17 = bf16[2,256]{1,0:T(2,128)(2,1)} copy(bf16[2,256]{1,0:T(2,128)(2,1)} %get-tuple-element.8) | data formatting | bytes 2048

commit v2 on v1

v2 whole, which is shorter than its diff:
```python
import functools

import jax
import jax.numpy as jnp
from jax import lax
from jax.experimental import pallas as pl
from jax.experimental.pallas import tpu as pltpu
from jax.sharding import PartitionSpec as P

HD = 64
CORES = 2

epsilon = 1e-06
masked_score = -1e30
MESH = pl.DeviceIdType.MESH


def kernel(
    dims,
    tok_hbm, gain_hbm, wk_hbm, wv_hbm, gates_hbm, q_hbm, nk_hbm, nv_hbm, ng_hbm,
    kbuf, vbuf, ro_ref,
    tok, inv, nb, acc, wbuf, gain_v, gain_row, gates_v, q_v, nk_v, nv_v, ng_v, stats,
    loc_sem, w_sem, small_sem, hop_sem,
    sx_sem, rx_sem, sp_sem, rp_sem, sr_sem, rr_sem, sz_sem, rz_sem,
):
    S, L, R, T, Z = dims
    X = T // CORES
    rows_each, D = tok.shape
    NC, KC = nb.shape[1], nb.shape[3]
    blocks = rows_each // R
    C = kbuf.shape[2]
    H = C // HD
    BL = T * L
    tp = lax.axis_index("tp")
    z = lax.axis_index("sp")
    x, c = tp // CORES, tp % CORES
    partner = x * CORES + (CORES - 1 - c)

    def rows(j):
        return pl.ds(j * R, R)

    loads = [pltpu.make_async_copy(tok_hbm.at[rows(j)], tok.at[rows(j)], loc_sem.at[j]) for j in range(blocks)]
    for copy in loads:
        copy.start()
    w_copies = [
        pltpu.make_async_copy(wk_hbm, wbuf.at[:, pl.ds(0, C)], w_sem.at[0]),
        pltpu.make_async_copy(wv_hbm, wbuf.at[:, pl.ds(C, C)], w_sem.at[1]),
    ]
    small = [
        pltpu.make_async_copy(src, dst, small_sem.at[i])
        for i, (src, dst) in enumerate(
            [(gain_hbm, gain_v), (gates_hbm, gates_v), (q_hbm, q_v), (nk_hbm, nk_v), (nv_hbm, nv_v), (ng_hbm, ng_v)]
        )
    ]
    for copy in small:
        copy.start()
    barrier = pltpu.get_barrier_semaphore()
    pl.semaphore_signal(barrier, inc=1, device_id={"tp": partner}, device_id_type=MESH)
    for d in range(1, X):
        pl.semaphore_signal(
            barrier, inc=1, device_id={"tp": ((x + d) % X) * CORES + c}, device_id_type=MESH
        )
    sides = (z > 0).astype(jnp.int32) + (z < Z - 1).astype(jnp.int32)

    def greet_sides(sem):
        @pl.when(z > 0)
        def _():
            pl.semaphore_signal(sem, inc=1, device_id={"sp": z - 1}, device_id_type=MESH)

        @pl.when(z < Z - 1)
        def _():
            pl.semaphore_signal(sem, inc=1, device_id={"sp": z + 1}, device_id_type=MESH)

    greet_sides(barrier)

    small[0].wait()
    g = gain_v[...].astype(jnp.float32)
    lanes = g.shape[1]
    for i in range(g.shape[0]):
        gain_row[:, pl.ds(i * lanes, lanes)] = g[i : i + 1, :]
    for j in range(blocks):
        loads[j].wait()
        if j == blocks - 1:
            for copy in w_copies:
                copy.start()
        v = tok[rows(j), :].astype(jnp.float32)
        r = lax.rsqrt(jnp.mean(v * v, axis=-1, keepdims=True) + epsilon)
        inv[rows(j), :] = jnp.broadcast_to(r, (R, KC))

    def x_copy(d, j):
        return pltpu.make_async_remote_copy(
            nb.at[tp, j], nb.at[tp, j], sx_sem.at[d - 1, j], rx_sem.at[d - 1, j],
            device_id={"tp": ((x + d) % X) * CORES + c}, device_id_type=MESH,
        )

    def x_source(d, core):
        return ((x + X - d) % X) * CORES + core

    def relay_copy(d, j):
        t = x_source(d, c)
        return pltpu.make_async_remote_copy(
            nb.at[t, j], nb.at[t, j], sr_sem.at[d - 1, j], rr_sem.at[d - 1, j],
            device_id={"tp": partner}, device_id_type=MESH,
        )

    def arrival(t, j, sem):
        return pltpu.make_async_remote_copy(
            nb.at[t, j], nb.at[t, j], sem, sem,
            device_id={"tp": partner}, device_id_type=MESH,
        )

    def norm(k):
        part = pl.ds(k * KC, KC)
        v = tok[:, part].astype(jnp.float32)
        nb[tp, k] = (v * inv[...] * gain_row[:, part]).astype(jnp.bfloat16)

    norm(0)
    norm(1)
    pl.semaphore_wait(barrier, 1 + (X - 1) + sides)
    for k in range(NC):
        for d in range(1, X):
            x_copy(d, k).start()
        if k + 2 < NC:
            norm(k + 2)
    own_to_partner = pltpu.make_async_remote_copy(
        nb.at[tp], nb.at[tp], sp_sem, rp_sem, device_id={"tp": partner}, device_id_type=MESH
    )
    own_to_partner.start()
    if Z > 2:
        greet_sides(hop_sem.at[0])

    for copy in small[1:]:
        copy.wait()
    acc[...] = jnp.zeros_like(acc)

    def project(group, k, first, second):
        part = pl.ds(pl.multiple_of(k * KC, KC), KC)
        both = jnp.concatenate([nb[first, k], nb[second, k]], axis=0)
        acc[group] += jnp.dot(both, wbuf[part, :], preferred_element_type=jnp.float32)

    def keep(group, first, second):
        for i, t in enumerate((first, second)):
            for s in range(S):
                y = acc[group, pl.ds(i * rows_each + s * L, L), :].astype(jnp.bfloat16)
                at = pl.ds(pl.multiple_of(t * L, L), L)
                kbuf[s, at, :] = y[:, :C]
                vbuf[s, at, :] = y[:, C:]

    for copy in w_copies:
        copy.wait()
    pltpu.make_async_remote_copy(
        nb.at[partner], nb.at[partner], sp_sem, rp_sem, device_id={"tp": partner}, device_id_type=MESH
    ).wait_recv()

    def near(k, carry):
        project(0, k, tp, partner)
        return carry

    lax.fori_loop(0, NC, near, 0)
    keep(0, tp, partner)
    for r in range(1, Z - 2):
        pl.semaphore_wait(hop_sem.at[r - 1], sides)
        greet_sides(hop_sem.at[r])

    def arrive(k):
        for d in range(1, X):
            arrival(x_source(d, c), k, rx_sem.at[d - 1, k]).wait_recv()
            relay_copy(d, k).start()

    def use(k):
        for d in range(1, X):
            first, second = x_source(d, c), x_source(d, CORES - 1 - c)
            arrival(second, k, rr_sem.at[d - 1, k]).wait_recv()
            project(d, k, first, second)

    def far(k, carry):
        arrive(k)
        use(k - 1)
        return carry

    arrive(0)
    lax.fori_loop(1, NC, far, 0)
    use(NC - 1)
    for d in range(1, X):
        keep(d, x_source(d, c), x_source(d, CORES - 1 - c))

    scale = HD ** (-0.5)
    head_of_lane = lax.broadcasted_iota(jnp.int32, (H, C), 1) // HD
    own_head = head_of_lane == lax.broadcasted_iota(jnp.int32, (H, C), 0)
    eye = lax.broadcasted_iota(jnp.int32, (H, H), 0) == lax.broadcasted_iota(jnp.int32, (H, H), 1)
    last_block = z == Z - 1

    def as_row(column):
        return jnp.sum(jnp.where(own_head, column, 0.0), axis=0, keepdims=True)

    for s in range(S):
        qd = jnp.where(own_head, q_v[s : s + 1, :].astype(jnp.float32), 0.0)
        fresh = jnp.sum(qd * nk_v[s : s + 1, :].astype(jnp.float32), axis=1, keepdims=True) * scale
        gates = gates_v[s]
        own_gate = jnp.sum(jnp.where(eye, ng_v[s : s + 1, :], 0.0), axis=1, keepdims=True)
        fresh = jnp.where(last_block, fresh - (gates[:, BL - 1 : BL] + own_gate), masked_score)
        scores = lax.dot_general(
            qd.astype(jnp.bfloat16), kbuf[s], (((1,), (1,)), ((), ())), preferred_element_type=jnp.float32
        )
        scores = scores * scale - gates
        top = jnp.maximum(jnp.max(scores, axis=1, keepdims=True), fresh)
        weights = jnp.exp(scores - top)
        fresh_weight = jnp.exp(fresh - top)
        total = jnp.sum(weights, axis=1, keepdims=True) + fresh_weight
        high = weights.astype(jnp.bfloat16)
        low = (weights - high.astype(jnp.float32)).astype(jnp.bfloat16)
        values = vbuf[s]
        weighted = jnp.dot(high, values, preferred_element_type=jnp.float32)
        weighted = weighted + jnp.dot(low, values, preferred_element_type=jnp.float32)
        weighted = weighted + fresh_weight * nv_v[s : s + 1, :].astype(jnp.float32)
        stats[z, 0, s : s + 1, :] = as_row(top)
        stats[z, 1, s : s + 1, :] = as_row(total)
        stats[z, 2, s : s + 1, :] = as_row(weighted)

    def z_copy(d):
        return pltpu.make_async_remote_copy(
            stats.at[z], stats.at[z], sz_sem.at[d - 1], rz_sem.at[d - 1],
            device_id={"sp": (z + d) % Z}, device_id_type=MESH,
        )

    if Z > 2:
        pl.semaphore_wait(hop_sem.at[Z - 3], sides)
    for d in range(1, Z):
        z_copy(d).start()
    for d in range(1, X):
        for j in range(NC):
            x_copy(d, j).wait_send()
            relay_copy(d, j).wait_send()
    own_to_partner.wait_send()
    for d in range(1, Z):
        source = (z + Z - d) % Z
        pltpu.make_async_remote_copy(
            stats.at[source], stats.at[source], sz_sem.at[d - 1], rz_sem.at[d - 1],
            device_id={"sp": source}, device_id_type=MESH,
        ).wait_recv()
    everything = stats[...]
    tops, totals, sums = everything[:, 0], everything[:, 1], everything[:, 2]
    factor = jnp.exp(tops - jnp.max(tops, axis=0, keepdims=True))
    ro_ref[...] = (jnp.sum(sums * factor, axis=0) / jnp.sum(totals * factor, axis=0)).astype(ro_ref.dtype)
    for d in range(1, Z):
        z_copy(d).wait_send()


def write_out(*refs):
    sems = refs[-1]
    count = (len(refs) - 1) // 2
    copies = [pltpu.make_async_copy(refs[i], refs[count + i], sems.at[i]) for i in range(count)]
    for copy in copies:
        copy.start()
    for copy in copies:
        copy.wait()


def body(
    tokens, norm_gain, key_weight, value_weight, cum_gates, new_query, new_key, new_value, new_gate
):
    S, L, D = tokens.shape
    C = key_weight.shape[1]
    H = C // HD
    T = lax.axis_size("tp")
    Z = lax.axis_size("sp")
    X = T // CORES
    BL = T * L
    R = 16 if L % 16 == 0 else L
    KC = 256 if D % 256 == 0 else D // 2
    NC = D // KC
    bf, f32 = jnp.bfloat16, jnp.float32
    hbm = pl.BlockSpec(memory_space=pltpu.HBM)
    dma = pltpu.SemaphoreType.DMA
    far = max(X - 1, 1)
    vmem = pl.BlockSpec(memory_space=pltpu.VMEM)
    results = pl.pallas_call(
        functools.partial(kernel, (S, L, R, T, Z)),
        out_shape=(
            pltpu.VMEM((S, BL, C), bf),
            pltpu.VMEM((S, BL, C), bf),
            pltpu.VMEM((S, C), bf),
        ),
        in_specs=[hbm] * 9,
        out_specs=(vmem, vmem, vmem),
        scratch_shapes=[
            pltpu.VMEM((S * L, D), bf),
            pltpu.VMEM((S * L, KC), f32),
            pltpu.VMEM((T, NC, S * L, KC), bf),
            pltpu.VMEM((X, 2 * S * L, 2 * C), f32),
            pltpu.VMEM((D, 2 * C), bf),
            pltpu.VMEM((D // 128, 128), bf),
            pltpu.VMEM((1, D), f32),
            pltpu.VMEM((S, H, BL), f32),
            pltpu.VMEM((S, C), bf),
            pltpu.VMEM((S, C), bf),
            pltpu.VMEM((S, C), bf),
            pltpu.VMEM((S, H), f32),
            pltpu.VMEM((Z, 3, S, C), f32),
            dma((S * L // R,)), dma((2,)), dma((6,)), pltpu.SemaphoreType.REGULAR((max(Z - 2, 1),)),
            dma((far, NC)), dma((far, NC)), dma, dma,
            dma((far, NC)), dma((far, NC)), dma((max(Z - 1, 1),)), dma((max(Z - 1, 1),)),
        ],
        compiler_params=pltpu.CompilerParams(
            collective_id=0, has_side_effects=True, vmem_limit_bytes=56 * 1024 * 1024
        ),
    )(
        tokens.reshape(S * L, D),
        norm_gain.reshape(D // 128, 128),
        key_weight,
        value_weight,
        jnp.transpose(cum_gates, (0, 2, 1)),
        new_query,
        new_key,
        new_value,
        new_gate,
    )
    return pl.pallas_call(
        write_out,
        out_shape=tuple(jax.ShapeDtypeStruct(r.shape, r.dtype) for r in results),
        in_specs=[vmem] * 3,
        out_specs=(hbm, hbm, hbm),
        scratch_shapes=[dma((3,))],
    )(*(pltpu.with_memory_space_constraint(r, pltpu.VMEM) for r in results))


def solution(mesh):
    in_specs = (
        P("gr", ("sp", "tp"), None),
        P(),
        P(None, "tp"),
        P(None, "tp"),
        P("gr", "sp", "tp"),
        P("gr", "tp"),
        P("gr", "tp"),
        P("gr", "tp"),
        P("gr", "tp"),
    )
    out_specs = (P("gr", "sp", "tp"), P("gr", "sp", "tp"), P("gr", "tp"))
    return jax.shard_map(body, mesh=mesh, in_specs=in_specs, out_specs=out_specs, check_vma=False)
```

time: 42.7 us -> 37 us (0.87)
  local copies, waits for them, and re-layouts: 5.85 us -> 0 us
    unnamed x3 -> x0, local copies, waits for them, and re-layouts: 4.54 us -> none
    reshape x1 -> x0, local copies, waits for them, and re-layouts: 1.31 us -> none  [body(): norm_gain.reshape(1, D)]
    pallas_call x1 -> x2, Pallas kernels: 36 us -> 36.3 us  [the longest x1 35.4 us: body(): pl.pallas_call(functools.partial(kernel, (S, L, R, T, Z)), out_shape=(plt...]
where the time goes in v2:
time: 37 us; the launch traced here: 36.9 us
  Pallas kernels  36.3 us (98%)
  between operations  0.64 us (2%)
    pallas_call x1, Pallas kernels, body(): pl.pallas_call(functools.partial(kernel, (S, L, R, T, Z)), out_shape=(plt...  35.4 us
    pallas_call x1, Pallas kernels, body(): pl.pallas_call(write_out, out_shape=tuple((jax.ShapeDtypeStruct(r.shape,...  0.82 us

profile of v2, /device:TPU:0, one launch (start us, length us, event | category | flops | bytes accessed | tf_op | source)
XLA Modules:
  0.0 36.9 jit_solution(4195655821460762547)
XLA Ops:
  0.6 35.4 %shard_map.112 = (bf16[2,256,256]{2,1,0:T(8,128)(2,1)S(1)}, bf16[2,256,256]{2,1,0:T(8,128)(2,1)S(1)}, bf16[2,256]{1,0:T(2,128)(2,1)S(1)}) custom-call(bf16[128,4096]{1,0:T(8,128)(2,1)} %bitcast.3, bf16[32,128]{1,0:T(8,128)(2,1)} %bitcast.4, bf16[4096,256]{1,0:T(8,128)(2,1)} %wk_hbm.1, bf16[4096,256]{1,0:T(8,128)(2,1)} %wv_hbm.1, f32[2,4,256]{2,1,0:T(4,128)} %bitcast.5, ...), custom_call_target="tpu_custom_call" | custom-call | tf_op jit(solution)/shard_map/pallas_call | solution.py:277
  36.1 0.8 %shard_map.113 = (bf16[2,256,256]{2,1,0:T(8,128)(2,1)}, bf16[2,256,256]{2,1,0:T(8,128)(2,1)}, bf16[2,256]{1,0:T(2,128)(2,1)}) custom-call(bf16[2,256,256]{2,1,0:T(8,128)(2,1)S(1)} %get-tuple-element.6.refs_0_, bf16[2,256,256]{2,1,0:T(8,128)(2,1)S(1)} %get-tuple-element.7.refs_1_, bf16[2,256]{1,0:T(2,128)(2,1)S(1)} %get-tuple-element.8.refs_2_), custom_call_target="tpu_custom_call" | custom-call | tf_op jit(solution)/shard_map/pallas_call | solution.py:318
